TPU v7x, 32 devices: a whole 2x2x4 slice. The times are simulated.
32 devices in a mesh: grp: 2 (over y), sp: 4 (over z), tp: 4 (over x, core).
Axes of the slice: x: 2, y: 2, z: 4, core: 2. Of those that a mesh axis runs over, the one named last changes fastest.
Arguments:
- queries: bfloat16 [2048, 1024], P(('grp', 'sp'), 'tp'), parts along dimension 0, may hold values from -7 to 10
- keys: bfloat16 [2048, 1024], P(('grp', 'sp'), 'tp'), parts along dimension 0, may hold values from -14 to 7
- values: bfloat16 [2048, 1024], P(('grp', 'sp'), 'tp'), parts along dimension 0, may hold values from -6 to 6
- resid: bfloat16 [2048, 2048], P(('grp', 'sp', 'tp')), parts along dimension 0, may hold values from -18 to 18
- out_weight: bfloat16 [1024, 2048], P('tp'), may hold values from -0.375 to 0.375
- gate_weight: bfloat16 [2048, 3072], P('sp', 'tp'), may hold values from -0.125 to 0.125
- value_weight: bfloat16 [2048, 3072], P('sp', 'tp'), may hold values from -0.125 to 0.125
- conv_gate: float32 [3, 3072], P(None, 'tp'), may hold values from -3 to 3
- conv_value: float32 [3, 3072], P(None, 'tp'), may hold values from -3 to 3
- norm_gain: float32 [2048], replicated, may hold values from 0.1 to 1.9
- down_weight: bfloat16 [3072, 2048], P('tp', 'sp'), may hold values from -0.109375 to 0.109375
Outputs:
- layer_out: bfloat16 [2048, 2048], P(('grp', 'sp', 'tp')), parts along dimension 0
There are 2 independent parts, one for each index of `grp`. A program takes and returns all parts, laid end to end along the dimension named above; an argument that names none is the same for every part. Nothing has to cross between parts.
All inputs are finite; a program needn't handle non-finite values.
Results may differ from a plain program's by a relative error of at most 0.0058.
Values may be sent and summed in bfloat16 or wider, within the bound.
A program may use at most 128 MiB of HBM per device.

v0:
```python
import jax
import jax.numpy as jnp
from jax import lax
from jax.sharding import PartitionSpec as P

HEAD = 64
epsilon = 1e-06


def shifted(block, axis, distance):
    devices = range(lax.axis_size(axis))
    route = [(i - distance, i) for i in devices if i - distance in devices]
    return lax.ppermute(block, axis, route)


def block_terms(query_rows, key_rows, value_rows, query_place, key_place):
    scores = jnp.einsum(
        "qhe,khe->hqk", query_rows, key_rows, preferred_element_type=jnp.float32
    ) * HEAD ** (-0.5)
    causal = (key_place[None, :] < query_place[:, None])[None]
    stay_log = jnp.where(causal, jax.nn.log_sigmoid(-scores), 0.0)
    suffix = lax.cumsum(stay_log, axis=2, reverse=True) - stay_log
    local_weight = jnp.where(causal, jnp.exp(jax.nn.log_sigmoid(scores) + suffix), 0.0).astype(
        jnp.bfloat16
    )
    part = jnp.einsum("hqk,khe->hqe", local_weight, value_rows, preferred_element_type=jnp.float32)
    return (jnp.sum(stay_log, axis=2), part)


def normalize(state, norm_gain):
    values = state.astype(jnp.float32)
    scaled = values * lax.rsqrt(jnp.mean(values * values, axis=-1, keepdims=True) + epsilon)
    return (scaled * norm_gain).astype(jnp.bfloat16)


def causal_conv(rim_rows, rows, taps):
    extended = jnp.concatenate([rim_rows, rows], axis=0).astype(jnp.float32)
    length = rows.shape[0]
    total = jnp.zeros(rows.shape, jnp.float32)
    for start_displacement in range(taps.shape[0]):
        total = (
            total
            + taps[start_displacement] * extended[start_displacement : start_displacement + length]
        )
    return total


def body(
    queries,
    keys,
    values,
    resid,
    out_weight,
    gate_weight,
    value_weight,
    conv_gate,
    conv_value,
    norm_gain,
    down_weight,
):
    tok_dev = queries.shape[0]
    mix_local = queries.shape[1]
    head_count = mix_local // HEAD
    sp_count = lax.axis_size("sp")
    block = tok_dev * min(sp_count, max(1, 1024 // tok_dev))
    paired = jnp.concatenate([keys, values], axis=1)
    gathered = lax.all_gather(paired, "sp", axis=0, tiled=True)
    mine = lax.axis_index("sp")
    query_place = mine * tok_dev + jnp.arange(tok_dev, dtype=jnp.int32)
    query_rows = queries.reshape(tok_dev, head_count, HEAD)

    def add_block(index, carry):
        start = index * block
        piece = lax.dynamic_slice_in_dim(gathered, start, block, 0)
        key_rows = piece[:, :mix_local].reshape(block, head_count, HEAD)
        value_rows = piece[:, mix_local:].reshape(block, head_count, HEAD)
        key_place = start + jnp.arange(block, dtype=jnp.int32)
        total, part = block_terms(query_rows, key_rows, value_rows, query_place, key_place)
        return carry * jnp.exp(total)[:, :, None] + part

    start_carry = jnp.zeros((head_count, tok_dev, HEAD), jnp.float32)
    attended = lax.fori_loop(0, mine * tok_dev // block + 1, add_block, start_carry)
    mixed = jnp.transpose(attended, (1, 0, 2)).reshape(tok_dev, mix_local).astype(jnp.bfloat16)
    projected = lax.psum_scatter(
        jnp.dot(mixed, out_weight, preferred_element_type=jnp.float32),
        "tp",
        scatter_dimension=0,
        tiled=True,
    )
    state = (resid.astype(jnp.float32) + projected).astype(jnp.bfloat16)
    normed = lax.all_gather(normalize(state, norm_gain), "tp", axis=0, tiled=True)
    ff_local = gate_weight.shape[1]
    gate_full = jnp.dot(
        normed,
        lax.all_gather(gate_weight, "sp", axis=0, tiled=True),
        preferred_element_type=jnp.float32,
    )
    value_full = jnp.dot(
        normed,
        lax.all_gather(value_weight, "sp", axis=0, tiled=True),
        preferred_element_type=jnp.float32,
    )
    gate_pre = gate_full.astype(jnp.bfloat16)
    value_pre = value_full.astype(jnp.bfloat16)
    taps_count = conv_gate.shape[0]
    rim = jnp.concatenate(
        [gate_pre[tok_dev - taps_count + 1 :], value_pre[tok_dev - taps_count + 1 :]], axis=1
    )
    before = shifted(rim, "sp", 1)
    conv_gate_out = causal_conv(before[:, :ff_local], gate_pre, conv_gate)
    conv_value_out = causal_conv(before[:, ff_local:], value_pre, conv_value)
    gated = (jax.nn.silu(conv_gate_out) * conv_value_out).astype(jnp.bfloat16)
    partial_sum = jnp.dot(
        gated,
        lax.all_gather(down_weight, "sp", axis=1, tiled=True),
        preferred_element_type=jnp.float32,
    )
    ffn_share = lax.psum_scatter(partial_sum, "tp", scatter_dimension=0, tiled=True)
    return (state.astype(jnp.float32) + ffn_share).astype(jnp.bfloat16)


def solution(mesh):
    placed = (
        P(("grp", "sp"), "tp"),
        P(("grp", "sp"), "tp"),
        P(("grp", "sp"), "tp"),
        P(("grp", "sp", "tp"), None),
        P("tp", None),
        P("sp", "tp"),
        P("sp", "tp"),
        P(None, "tp"),
        P(None, "tp"),
        P(),
        P("tp", "sp"),
    )
    return jax.shard_map(
        body, mesh=mesh, in_specs=placed, out_specs=P(("grp", "sp", "tp"), None), check_vma=False
    )
```

profile of v0, /device:TPU:0, one launch (start us, length us, event | category | flops | bytes accessed | tf_op | source)
XLA Modules:
  0.0 383.4 jit_solution(949477178948924257)
XLA Ops:
  6.5 1.1 copy.14
  7.6 1.0 copy.15
  8.6 0.7 pad_maximum_fusion
  9.5 1.0 copy.16
  10.5 31.7 %all-gather.6.cloned.1.call-done = bf16[1024,512]{0,1:T(8,128)(2,1)} async-done(((bf16[256,512]{0,1:T(8,128)(2,1)}), bf16[1024,512]{0,1:T(8,128)(2,1)}) %all-gather.6.cloned.1.call-update) | async-done | bytes 1048592 | tf_op jit(solution)/shard_map/all_gather | solution.py:67
  42.2 56.0 %while.11 = (s32[]{:T(128)}, f32[4,256,64]{1,2,0:T(8,128)S(1)}, s32[]{:T(128)}, bf16[1024,512]{0,1:T(8,128)(2,1)}, bf16[256,4,64]{0,2,1:T(8,128)(2,1)S(1)}, /*index=5*/s32[]{:T(128)}, s32[]{:T(128)}, s32[]{:T(128)}, f32[]{:T(128)}) while((s32[]{:T(128)}, f32[4,256,64]{1,2,0:T(8,128)S(1)}, s32[]{:T(128)}, ...), condition=%wide.region_4.5_spmd.clone, body=%wide.region_0.4_spmd.clone.sunk | while | flops 447937792 | bytes 93714576 | solution.py:82
  42.2 1.3 fusion.66
  43.5 2.9 fusion.67
  46.6 5.6 %fusion.68 = (f32[4,256]{1,0:T(4,128)S(1)}, f32[4,256,1024]{2,1,0:T(8,128)S(1)}) fusion(f32[4,256,1024]{2,1,0:T(8,128)} %get-tuple-element.134, u8[256,1024]{1,0:T(8,128)(4,1)S(1)} %get-tuple-element.135, pred[256,1024]{1,0:T(8,128)(4,1)S(1)} %broadcast_compare_fusion.2), kind=kLoop, calls=%fused_computation.20.clone.1 | loop fusion | flops 13630464 | bytes 8916992 | tf_op jit(solution)/shard_map/while/body/reduce_sum | solution.py:27
  52.3 3.0 copy.21
  55.2 5.5 %copy.22 = f32[4,256,8,128]{1,2,3,0:T(8,128)} copy(f32[4,256,8,128]{3,2,1,0:T(8,128)} %bitcast.44) | data formatting | bytes 8388608 | tf_op jit(solution)/shard_map/reshape
  60.8 10.8 %fusion.69 = f32[4,256,8,128]{1,2,3,0:T(8,128)S(1)} fusion(f32[4,256,8,128]{1,2,3,0:T(8,128)} %copy.22), kind=kOutput, calls=%fused_computation.65.clone.1 | output fusion | flops 133169152 | bytes 8388608 | tf_op jit(solution)/shard_map/reduce-window
  71.6 2.0 copy-done.1
  73.6 4.5 %broadcast_add_fusion.2 = f32[4,256,8,128]{1,2,3,0:T(8,128)} fusion(f32[4,256,8,128]{1,2,3,0:T(8,128)} %copy-done.1, f32[4,256,8]{1,2,0:T(8,128)S(1)} %slice.148), kind=kLoop, calls=%fused_computation.10.clone.1 | loop fusion | flops 1048576 | bytes 8421376 | tf_op jit(solution)/shard_map/reduce_window_sum | solution.py:22
  78.1 5.5 %copy.23 = f32[4,256,8,128]{3,2,1,0:T(8,128)} copy(f32[4,256,8,128]{1,2,3,0:T(8,128)} %broadcast_add_fusion.2) | data formatting | bytes 8388608 | tf_op jit(solution)/shard_map/reduce_window_sum | solution.py:22
  83.6 4.9 %reduce_window_sum.20 = f32[4,256,1024]{2,1,0:T(8,128)} reshape(f32[4,256,8,128]{3,2,1,0:T(8,128)} %copy.23) | data formatting | bytes 8388608 | tf_op jit(solution)/shard_map/reduce_window_sum | solution.py:22
  88.5 9.5 %fusion.70 = f32[4,256,64]{1,2,0:T(8,128)S(1)} fusion(bf16[1024,4,64]{0,2,1:T(8,128)(2,1)S(1)} %bitcast.46, f32[4,256,1024]{2,1,0:T(8,128)} %reduce_window_sum.20, f32[4,256,1024]{2,1,0:T(8,128)} %get-tuple-element.134, pred[256,1024]{1,0:T(8,128)(4,1)S(1)} %broadcast_compare_fusion.2, f32[4,256,64]{1,2,0:T(8,128)S(1)} %get-tuple-element.148, ...), kind=kOutput, calls=%fused_computation.12.clone.1 | convolution fusion | flops 159514624 | bytes 9965568 | tf_op jit(solution)/shard_map/while/body/hqk,khe->hqe/dot_general | solution.py:26
  98.3 1.8 fusion.39
  100.9 28.8 %reduce-scatter.3.cloned.1.call-done = f32[64,2048]{1,0:T(8,128)} async-done(((f32[256,2048]{1,0:T(8,128)}), f32[64,2048]{1,0:T(8,128)}) %reduce-scatter.3.cloned.1.call-update) | async-done | bytes 524304 | tf_op jit(solution)/shard_map/reduce_scatter | solution.py:84
  129.8 1.2 fusion.22
  131.0 0.8 fusion.24
  133.1 61.7 %all-gather.10.cloned.1.call-done = bf16[2048,768]{1,0:T(8,128)(2,1)} async-done(((bf16[512,768]{1,0:T(8,128)(2,1)}), bf16[2048,768]{1,0:T(8,128)(2,1)}) %all-gather.10.cloned.1.call-update) | async-done | bytes 3145744 | tf_op jit(solution)/shard_map/all_gather | solution.py:95
  194.8 16.8 %all-gather.8.cloned.1.call-done = bf16[256,2048]{1,0:T(8,128)(2,1)} async-done(((bf16[64,2048]{1,0:T(8,128)(2,1)}), bf16[256,2048]{1,0:T(8,128)(2,1)}) %all-gather.8.cloned.1.call-update) | async-done | bytes 1048592 | tf_op jit(solution)/shard_map/all_gather | solution.py:91
  211.6 3.3 convolution_convert_fusion.1
  215.0 61.6 %all-gather.12.cloned.1.call-done = bf16[2048,768]{1,0:T(8,128)(2,1)} async-done(((bf16[512,768]{1,0:T(8,128)(2,1)}), bf16[2048,768]{1,0:T(8,128)(2,1)}) %all-gather.12.cloned.1.call-update) | async-done | bytes 3145744 | tf_op jit(solution)/shard_map/all_gather | solution.py:100
  276.5 2.9 convolution_convert_fusion
  279.4 1.3 collective-permute-start
  280.8 1.2 collective-permute-done
  282.2 57.8 %all-gather.14.cloned.1.call-done = bf16[768,2048]{1,0:T(8,128)(2,1)} async-done(((bf16[768,512]{1,0:T(8,128)(2,1)}), bf16[768,2048]{1,0:T(8,128)(2,1)}) %all-gather.14.cloned.1.call-update) | async-done | bytes 3145744 | tf_op jit(solution)/shard_map/all_gather | solution.py:115
  340.1 4.7 %fusion.26 = f32[256,2048]{1,0:T(8,128)} fusion(bf16[768,2048]{1,0:T(8,128)(2,1)} %all-gather.14.cloned.1.call-done, f32[258,768]{1,0:T(8,128)S(1)} %get-tuple-element.84, f32[258,768]{1,0:T(8,128)S(1)} %get-tuple-element.83, f32[768]{0:T(1024)S(1)} %get-tuple-element.59, f32[768]{0:T(1024)S(1)} %get-tuple-element.60, f32[768]{0:T(1024)S(1)} %get-tuple-element.58, ...), kind=kOutput, calls=%fused_computation.45 | convolution fusion | flops 808452096 | bytes 9986048 | tf_op jit(solution)/shard_map/dot_general | solution.py:113
  344.8 30.0 %reduce-scatter.5.cloned.1.call-done = f32[64,2048]{1,0:T(8,128)} async-done(((f32[256,2048]{1,0:T(8,128)}), f32[64,2048]{1,0:T(8,128)}) %reduce-scatter.5.cloned.1.call-update) | async-done | bytes 524304 | tf_op jit(solution)/shard_map/reduce_scatter | solution.py:118
  374.8 1.8 fusion.25
  (43 shorter events, 2.7 us)
Async XLA Ops:
  6.5 91.8 %copy-start = (bf16[256,2048]{1,0:T(8,128)(2,1)S(1)}, bf16[256,2048]{1,0:T(8,128)(2,1)}, u32[]{:S(2)}) copy-start(bf16[256,2048]{1,0:T(8,128)(2,1)} %param.17) | copy-start | bytes 3145732
  6.5 35.7 %all-gather.6.cloned.1.call-start = ((), (), s32[]{:S(2)}) async-start(), calls=%async_computation.2 | async-start | bytes 1310720 | tf_op jit(solution)/shard_map/all_gather | solution.py:67
  9.4 120.4 %reduce-scatter.3.cloned.1.call-start = ((), (), s32[]{:S(2)}) async-start(), calls=%async_computation.3 | async-start | bytes 2621440 | tf_op jit(solution)/shard_map/reduce_scatter | solution.py:84
  71.6 2.0 copy-start.1
  98.2 31.5 %copy-start.2 = (bf16[64,2048]{1,0:T(8,128)(2,1)S(1)}, bf16[64,2048]{1,0:T(8,128)(2,1)}, u32[]{:S(2)}) copy-start(bf16[64,2048]{1,0:T(8,128)(2,1)} %param.16) | copy-start | bytes 786436
  98.3 32.8 %copy-start.3 = (f32[2048]{0:T(1024)S(1)}, f32[2048]{0:T(1024)}, u32[]{:S(2)}) copy-start(f32[2048]{0:T(1024)} %param.22) | copy-start | bytes 24580
  100.2 94.7 %all-gather.10.cloned.1.call-start = ((), (), s32[]{:S(2)}) async-start(), calls=%async_computation.5 | async-start | bytes 3932160 | tf_op jit(solution)/shard_map/all_gather | solution.py:95
  100.9 110.7 %all-gather.8.cloned.1.call-start = ((), (), s32[]{:S(2)}) async-start(), calls=%async_computation.4 | async-start | bytes 1310720 | tf_op jit(solution)/shard_map/all_gather | solution.py:91
  131.9 144.6 %all-gather.12.cloned.1.call-start = ((), (), s32[]{:S(2)}) async-start(), calls=%async_computation.6 | async-start | bytes 3932160 | tf_op jit(solution)/shard_map/all_gather | solution.py:100
  132.5 207.6 %all-gather.14.cloned.1.call-start = ((), (), s32[]{:S(2)}) async-start(), calls=%async_computation.7 | async-start | bytes 3932160 | tf_op jit(solution)/shard_map/all_gather | solution.py:115
  133.1 241.7 %reduce-scatter.5.cloned.1.call-start = ((), (), s32[]{:S(2)}) async-start(), calls=%async_computation.8 | async-start | bytes 2621440 | tf_op jit(solution)/shard_map/reduce_scatter | solution.py:118
  211.6 64.9 %copy-start.6 = (bf16[256,2048]{1,0:T(8,128)(2,1)S(1)}, bf16[256,2048]{1,0:T(8,128)(2,1)}, u32[]{:S(2)}) copy-start(bf16[256,2048]{1,0:T(8,128)(2,1)} %all-gather.8.cloned.1.call-done) | copy-start | bytes 3145732
  214.9 65.8 %copy-start.4 = (f32[3,768]{1,0:T(4,128)S(1)}, f32[3,768]{1,0:T(4,128)}, u32[]{:S(2)}) copy-start(f32[3,768]{1,0:T(4,128)} %param.21) | copy-start | bytes 27652
  214.9 65.8 %copy-start.5 = (f32[3,768]{1,0:T(4,128)S(1)}, f32[3,768]{1,0:T(4,128)}, u32[]{:S(2)}) copy-start(f32[3,768]{1,0:T(4,128)} %param.20) | copy-start | bytes 27652
  279.4 2.6 collective-permute-start
Sparse Core Ops, SparseCore 0:
  9.5 32.6 all-gather.5
  100.3 29.4 reduce-scatter.2
  131.4 63.4 all-gather.9
  196.3 15.3 all-gather.7
  213.0 63.4 all-gather.11
  278.0 62.0 all-gather.13
  344.9 29.8 reduce-scatter.4
where the time goes:
time: 384 us; the launch traced here: 383 us
  waiting for transfers between devices  292 us (76%)
  other arithmetic  25.9 us (7%)
  local copies, waits for them, and re-layouts  25.4 us (7%)
  matrix products  25.1 us (7%)
  between operations  13.7 us (4%)
    all_gather x1, waiting for transfers between devices, body(): lax.all_gather(gate_weight, 'sp', axis=0, tiled=True)  61.7 us
    all_gather x1, waiting for transfers between devices, body(): lax.all_gather(value_weight, 'sp', axis=0, tiled=True)  61.6 us
    all_gather x1, waiting for transfers between devices, body(): lax.all_gather(down_weight, 'sp', axis=1, tiled=True)  57.8 us
    all_gather x1, waiting for transfers between devices, body(): gathered = lax.all_gather(paired, 'sp', axis=0, tiled=True)  31.7 us
    reduce_scatter x1, waiting for transfers between devices, body(): lax.psum_scatter(partial_sum, 'tp', scatter_dimension=0, tiled=True)  30 us
    reduce_scatter x1, waiting for transfers between devices, body(): lax.psum_scatter(jnp.dot(mixed, out_weight, preferred_element_type=jnp.fl...  28.8 us
    all_gather x1, waiting for transfers between devices, body(): lax.all_gather(normalize(state, norm_gain), 'tp', axis=0, tiled=True)  16.8 us
    another operation x2, other arithmetic  10.9 us
  transfers between devices with their start and end apart: 8, of which 8 were waited for; matrix products, arithmetic and copies ran while one was open for 2% of the time, Pallas kernels for 0%

commit v1 on v0

--- a/solution.py
+++ b/solution.py
@@ -64,7 +64,13 @@
     sp_count = lax.axis_size("sp")
     block = tok_dev * min(sp_count, max(1, 1024 // tok_dev))
     paired = jnp.concatenate([keys, values], axis=1)
-    gathered = lax.all_gather(paired, "sp", axis=0, tiled=True)
+    size = lax.axis_size("sp")
+    held, blocks = (paired, [paired])
+    for _ in range(size - 1):
+        held = lax.ppermute(held, "sp", [(i_2, (i_2 + 1) % size) for i_2 in range(size)])
+        blocks.insert(0, held)
+    merged = jnp.concatenate(blocks, axis=0)
+    gathered = jnp.roll(merged, (lax.axis_index("sp") + 1) * paired.shape[0], axis=0)
     mine = lax.axis_index("sp")
     query_place = mine * tok_dev + jnp.arange(tok_dev, dtype=jnp.int32)
     query_rows = queries.reshape(tok_dev, head_count, HEAD)

time: 384 us -> 351 us (0.914)
  waiting for transfers between devices: 292 us -> 253 us
    all_gather x1 -> x0, waiting for transfers between devices: 31.7 us -> none  [body(): gathered = lax.all_gather(paired, 'sp', axis=0, tiled=True)]
    all_gather x1, waiting for transfers between devices: 61.7 us -> 30.6 us  [body(): lax.all_gather(gate_weight, 'sp', axis=0, tiled=True)]
    ppermute x0 -> x3, waiting for transfers between devices: none -> 25 us  [body(): lax.ppermute(held, 'sp', [(i_2, (i_2 + 1) % size) for i_2 in range(size)])]
  transfers between devices with their start and end apart: 8 -> 10, of which waited for: 8 -> 10; matrix products, arithmetic and copies ran while one was open for 2% -> 3% of each run, Pallas kernels for 0% -> 0%
where the time goes in v1:
time: 351 us; the launch traced here: 350 us
  waiting for transfers between devices  253 us (72%)
  other arithmetic  26.3 us (7%)
  local copies, waits for them, and re-layouts  25.9 us (7%)
  matrix products  25.1 us (7%)
  between operations  15.3 us (4%)
  starting transfers between devices  4.61 us (1%)
    all_gather x1, waiting for transfers between devices, body(): lax.all_gather(value_weight, 'sp', axis=0, tiled=True)  61.5 us
    all_gather x1, waiting for transfers between devices, body(): lax.all_gather(down_weight, 'sp', axis=1, tiled=True)  57.9 us
    all_gather x1, waiting for transfers between devices, body(): lax.all_gather(gate_weight, 'sp', axis=0, tiled=True)  30.6 us
    reduce_scatter x1, waiting for transfers between devices, body(): lax.psum_scatter(partial_sum, 'tp', scatter_dimension=0, tiled=True)  30 us
    reduce_scatter x1, waiting for transfers between devices, body(): lax.psum_scatter(jnp.dot(mixed, out_weight, preferred_element_type=jnp.fl...  28.4 us
    ppermute x3, waiting for transfers between devices, body(): lax.ppermute(held, 'sp', [(i_2, (i_2 + 1) % size) for i_2 in range(size)])  25 us
    all_gather x1, waiting for transfers between devices, body(): lax.all_gather(normalize(state, norm_gain), 'tp', axis=0, tiled=True)  16.7 us
    another operation x2, other arithmetic  10.9 us
  transfers between devices with their start and end apart: 10, of which 10 were waited for; matrix products, arithmetic and copies ran while one was open for 3% of the time, Pallas kernels for 0%

profile of v1, /device:TPU:0, one launch (start us, length us, event | category | flops | bytes accessed | tf_op | source)
XLA Modules:
  0.0 350.2 jit_solution(15778537224083809191)
XLA Ops:
  7.4 1.1 copy.14
  8.5 1.0 copy.15
  9.5 3.1 collective-permute-start
  12.6 8.3 %collective-permute-done = bf16[256,512]{0,1:T(8,128)(2,1)S(1)} collective-permute-done((bf16[256,512]{0,1:T(8,128)(2,1)S(1)}, bf16[256,512]{0,1:T(8,128)(2,1)S(1)}, u32[]{:S(2)}, u32[]{:S(2)}) %collective-permute-start) | collective-permute-done | bytes 262176 | tf_op jit(solution)/shard_map/ppermute | solution.py:70
  20.9 9.3 %collective-permute-done.1 = bf16[256,512]{0,1:T(8,128)(2,1)S(1)} collective-permute-done((bf16[256,512]{0,1:T(8,128)(2,1)S(1)}, bf16[256,512]{0,1:T(8,128)(2,1)S(1)}, u32[]{:S(2)}, u32[]{:S(2)}) %collective-permute-start.1) | collective-permute-done | bytes 262176 | tf_op jit(solution)/shard_map/ppermute | solution.py:70
  31.2 7.4 %collective-permute-done.2 = bf16[256,512]{0,1:T(8,128)(2,1)S(1)} collective-permute-done((bf16[256,512]{0,1:T(8,128)(2,1)S(1)}, bf16[256,512]{0,1:T(8,128)(2,1)S(1)}, u32[]{:S(2)}, u32[]{:S(2)}) %collective-permute-start.2) | collective-permute-done | bytes 262176 | tf_op jit(solution)/shard_map/ppermute | solution.py:70
  39.7 55.4 %while.11 = (s32[]{:T(128)}, f32[4,256,64]{1,2,0:T(8,128)}, s32[]{:T(128)}, bf16[1024,512]{0,1:T(8,128)(2,1)S(1)}, bf16[256,4,64]{0,2,1:T(8,128)(2,1)S(1)}, /*index=5*/s32[]{:T(128)}, s32[]{:T(128)}, s32[]{:T(128)}, f32[]{:T(128)}) while((s32[]{:T(128)}, f32[4,256,64]{1,2,0:T(8,128)}, s32[]{:T(128)}, ...), condition=%wide.region_4.5_spmd.clone, body=%wide.region_0.4_spmd.clone.sunk | while | flops 447937792 | bytes 95811784 | solution.py:88
  39.8 2.9 fusion.67
  43.0 5.6 %fusion.68 = (f32[4,256]{1,0:T(4,128)S(1)}, f32[4,256,1024]{2,1,0:T(8,128)S(1)}) fusion(f32[4,256,1024]{2,1,0:T(8,128)} %get-tuple-element.134, u8[256,1024]{1,0:T(8,128)(4,1)S(1)} %get-tuple-element.135, pred[256,1024]{1,0:T(8,128)(4,1)S(1)} %broadcast_compare_fusion.2), kind=kLoop, calls=%fused_computation.20.clone.1 | loop fusion | flops 13630464 | bytes 8916992 | tf_op jit(solution)/shard_map/while/body/reduce_sum | solution.py:27
  48.6 3.0 copy.21
  51.5 5.6 %copy.22 = f32[4,256,8,128]{1,2,3,0:T(8,128)} copy(f32[4,256,8,128]{3,2,1,0:T(8,128)} %bitcast.44) | data formatting | bytes 8388608 | tf_op jit(solution)/shard_map/reshape
  57.1 10.8 %fusion.69 = f32[4,256,8,128]{1,2,3,0:T(8,128)S(1)} fusion(f32[4,256,8,128]{1,2,3,0:T(8,128)} %copy.22), kind=kOutput, calls=%fused_computation.74.clone.1 | output fusion | flops 133169152 | bytes 8388608 | tf_op jit(solution)/shard_map/reduce-window
  67.9 2.0 copy-done.1
  69.9 4.5 %broadcast_add_fusion.2 = f32[4,256,8,128]{1,2,3,0:T(8,128)} fusion(f32[4,256,8,128]{1,2,3,0:T(8,128)} %copy-done.1, f32[4,256,8]{1,2,0:T(8,128)S(1)} %slice.148), kind=kLoop, calls=%fused_computation.10.clone.1 | loop fusion | flops 1048576 | bytes 8421376 | tf_op jit(solution)/shard_map/reduce_window_sum | solution.py:22
  74.4 5.5 %copy.23 = f32[4,256,8,128]{3,2,1,0:T(8,128)} copy(f32[4,256,8,128]{1,2,3,0:T(8,128)} %broadcast_add_fusion.2) | data formatting | bytes 8388608 | tf_op jit(solution)/shard_map/reduce_window_sum | solution.py:22
  79.9 4.9 %reduce_window_sum.20 = f32[4,256,1024]{2,1,0:T(8,128)} reshape(f32[4,256,8,128]{3,2,1,0:T(8,128)} %copy.23) | data formatting | bytes 8388608 | tf_op jit(solution)/shard_map/reduce_window_sum | solution.py:22
  84.9 9.5 %fusion.70 = f32[4,256,64]{1,2,0:T(8,128)S(1)} fusion(bf16[1024,4,64]{0,2,1:T(8,128)(2,1)S(1)} %bitcast.46, f32[4,256,1024]{2,1,0:T(8,128)} %reduce_window_sum.20, f32[4,256,1024]{2,1,0:T(8,128)} %get-tuple-element.134, pred[256,1024]{1,0:T(8,128)(4,1)S(1)} %broadcast_compare_fusion.2, f32[4,256,64]{1,2,0:T(8,128)S(1)} %copy-done.2, ...), kind=kOutput, calls=%fused_computation.12.clone.1 | convolution fusion | flops 159514624 | bytes 9965568 | tf_op jit(solution)/shard_map/while/body/hqk,khe->hqe/dot_general | solution.py:26
  95.1 1.0 convert_element_type.44
  96.1 1.8 fusion.39
  98.6 28.4 %reduce-scatter.3.cloned.1.call-done = f32[64,2048]{1,0:T(8,128)} async-done(((f32[256,2048]{1,0:T(8,128)}), f32[64,2048]{1,0:T(8,128)}) %reduce-scatter.3.cloned.1.call-update) | async-done | bytes 524304 | tf_op jit(solution)/shard_map/reduce_scatter | solution.py:90
  127.1 1.2 fusion.22
  130.5 30.6 %all-gather.7.cloned.1.call-done = bf16[2048,768]{1,0:T(8,128)(2,1)} async-done(((bf16[512,768]{1,0:T(8,128)(2,1)}), bf16[2048,768]{1,0:T(8,128)(2,1)}) %all-gather.7.cloned.1.call-update) | async-done | bytes 3145744 | tf_op jit(solution)/shard_map/all_gather | solution.py:101
  161.2 16.7 %all-gather.5.cloned.1.call-done = bf16[256,2048]{1,0:T(8,128)(2,1)} async-done(((bf16[64,2048]{1,0:T(8,128)(2,1)}), bf16[256,2048]{1,0:T(8,128)(2,1)}) %all-gather.5.cloned.1.call-update) | async-done | bytes 1048592 | tf_op jit(solution)/shard_map/all_gather | solution.py:97
  177.8 3.3 convolution_convert_fusion.1
  181.1 61.5 %all-gather.9.cloned.1.call-done = bf16[2048,768]{1,0:T(8,128)(2,1)} async-done(((bf16[512,768]{1,0:T(8,128)(2,1)}), bf16[2048,768]{1,0:T(8,128)(2,1)}) %all-gather.9.cloned.1.call-update) | async-done | bytes 3145744 | tf_op jit(solution)/shard_map/all_gather | solution.py:106
  242.6 2.9 convolution_convert_fusion
  245.5 1.3 collective-permute-start.3
  246.9 1.2 collective-permute-done.3
  248.3 57.9 %all-gather.11.cloned.1.call-done = bf16[768,2048]{1,0:T(8,128)(2,1)} async-done(((bf16[768,512]{1,0:T(8,128)(2,1)}), bf16[768,2048]{1,0:T(8,128)(2,1)}) %all-gather.11.cloned.1.call-update) | async-done | bytes 3145744 | tf_op jit(solution)/shard_map/all_gather | solution.py:121
  306.2 4.7 %fusion.26 = f32[256,2048]{1,0:T(8,128)} fusion(bf16[768,2048]{1,0:T(8,128)(2,1)} %all-gather.11.cloned.1.call-done, f32[258,768]{1,0:T(8,128)S(1)} %get-tuple-element.84, f32[258,768]{1,0:T(8,128)S(1)} %get-tuple-element.83, f32[768]{0:T(1024)S(1)} %get-tuple-element.59, f32[768]{0:T(1024)S(1)} %get-tuple-element.60, f32[768]{0:T(1024)S(1)} %get-tuple-element.58, ...), kind=kOutput, calls=%fused_computation.45 | convolution fusion | flops 808452096 | bytes 9986048 | tf_op jit(solution)/shard_map/dot_general | solution.py:119
  310.9 30.0 %reduce-scatter.5.cloned.1.call-done = f32[64,2048]{1,0:T(8,128)} async-done(((f32[256,2048]{1,0:T(8,128)}), f32[64,2048]{1,0:T(8,128)}) %reduce-scatter.5.cloned.1.call-update) | async-done | bytes 524304 | tf_op jit(solution)/shard_map/reduce_scatter | solution.py:124
  340.8 1.8 fusion.25
  (59 shorter events, 6.2 us)
Async XLA Ops:
  7.4 88.8 %copy-start = (bf16[256,2048]{1,0:T(8,128)(2,1)S(1)}, bf16[256,2048]{1,0:T(8,128)(2,1)}, u32[]{:S(2)}) copy-start(bf16[256,2048]{1,0:T(8,128)(2,1)} %param.17) | copy-start | bytes 3145732
  7.4 119.7 %reduce-scatter.3.cloned.1.call-start = ((), (), s32[]{:S(2)}) async-start(), calls=%async_computation.2 | async-start | bytes 2621440 | tf_op jit(solution)/shard_map/reduce_scatter | solution.py:90
  9.5 11.4 %collective-permute-start = (bf16[256,512]{0,1:T(8,128)(2,1)S(1)}, bf16[256,512]{0,1:T(8,128)(2,1)S(1)}, u32[]{:S(2)}, u32[]{:S(2)}) collective-permute-start(bf16[256,512]{0,1:T(8,128)(2,1)S(1)} %pad_maximum_fusion), channel_id=1, source_target_pairs={{0,4},{4,8},{8,12},{12,0},{1,5},{5,9},{9,13},{13,1},{2,6},{6,10},{... | collective-permute-start | bytes 786440 | tf_op jit(solution)/shard_map/ppermute | solution.py:70
  20.9 9.3 %collective-permute-start.1 = (bf16[256,512]{0,1:T(8,128)(2,1)S(1)}, bf16[256,512]{0,1:T(8,128)(2,1)S(1)}, u32[]{:S(2)}, u32[]{:S(2)}) collective-permute-start(bf16[256,512]{0,1:T(8,128)(2,1)S(1)} %collective-permute-done), channel_id=1, source_target_pairs={{0,4},{4,8},{8,12},{12,0},{1,5},{5,9},{9,13},{13,1},{2,6},{6,10},{... | collective-permute-start | bytes 786440 | tf_op jit(solution)/shard_map/ppermute | solution.py:70
  30.2 8.4 %collective-permute-start.2 = (bf16[256,512]{0,1:T(8,128)(2,1)S(1)}, bf16[256,512]{0,1:T(8,128)(2,1)S(1)}, u32[]{:S(2)}, u32[]{:S(2)}) collective-permute-start(bf16[256,512]{0,1:T(8,128)(2,1)S(1)} %collective-permute-done.1), channel_id=1, source_target_pairs={{0,4},{4,8},{8,12},{12,0},{1,5},{5,9},{9,13},{13,1},{2,6},{6,10},{... | collective-permute-start | bytes 786440 | tf_op jit(solution)/shard_map/ppermute | solution.py:70
  67.9 2.0 copy-start.1
  79.9 5.0 %copy-start.2 = (f32[4,256,64]{1,2,0:T(8,128)S(1)}, f32[4,256,64]{1,2,0:T(8,128)}, u32[]{:S(2)}) copy-start(f32[4,256,64]{1,2,0:T(8,128)} %get-tuple-element.148) | copy-start | bytes 786436 | tf_op jit(solution)/shard_map/while
  94.4 0.7 copy-start.3
  95.1 31.9 %copy-start.4 = (bf16[64,2048]{1,0:T(8,128)(2,1)S(1)}, bf16[64,2048]{1,0:T(8,128)(2,1)}, u32[]{:S(2)}) copy-start(bf16[64,2048]{1,0:T(8,128)(2,1)} %param.16) | copy-start | bytes 786436
  95.1 33.2 %copy-start.5 = (f32[2048]{0:T(1024)S(1)}, f32[2048]{0:T(1024)}, u32[]{:S(2)}) copy-start(f32[2048]{0:T(1024)} %param.22) | copy-start | bytes 24580
  98.0 63.2 %all-gather.7.cloned.1.call-start = ((), (), s32[]{:S(2)}) async-start(), calls=%async_computation.4 | async-start | bytes 3932160 | tf_op jit(solution)/shard_map/all_gather | solution.py:101
  98.6 79.2 %all-gather.5.cloned.1.call-start = ((), (), s32[]{:S(2)}) async-start(), calls=%async_computation.3 | async-start | bytes 1310720 | tf_op jit(solution)/shard_map/all_gather | solution.py:97
  129.2 113.4 %all-gather.9.cloned.1.call-start = ((), (), s32[]{:S(2)}) async-start(), calls=%async_computation.5 | async-start | bytes 3932160 | tf_op jit(solution)/shard_map/all_gather | solution.py:106
  129.8 176.4 %all-gather.11.cloned.1.call-start = ((), (), s32[]{:S(2)}) async-start(), calls=%async_computation.6 | async-start | bytes 3932160 | tf_op jit(solution)/shard_map/all_gather | solution.py:121
  130.5 210.3 %reduce-scatter.5.cloned.1.call-start = ((), (), s32[]{:S(2)}) async-start(), calls=%async_computation.7 | async-start | bytes 2621440 | tf_op jit(solution)/shard_map/reduce_scatter | solution.py:124
  177.8 64.8 %copy-start.8 = (bf16[256,2048]{1,0:T(8,128)(2,1)S(1)}, bf16[256,2048]{1,0:T(8,128)(2,1)}, u32[]{:S(2)}) copy-start(bf16[256,2048]{1,0:T(8,128)(2,1)} %all-gather.5.cloned.1.call-done) | copy-start | bytes 3145732
  181.1 65.7 %copy-start.6 = (f32[3,768]{1,0:T(4,128)S(1)}, f32[3,768]{1,0:T(4,128)}, u32[]{:S(2)}) copy-start(f32[3,768]{1,0:T(4,128)} %param.21) | copy-start | bytes 27652
  181.1 65.7 %copy-start.7 = (f32[3,768]{1,0:T(4,128)S(1)}, f32[3,768]{1,0:T(4,128)}, u32[]{:S(2)}) copy-start(f32[3,768]{1,0:T(4,128)} %param.20) | copy-start | bytes 27652
  245.5 2.6 collective-permute-start.3
Sparse Core Ops, SparseCore 0:
  98.1 28.8 reduce-scatter.2
  311.0 29.7 reduce-scatter.4
Sparse Core Ops, SparseCore 1:
  100.0 61.0 all-gather.6
  162.6 15.2 all-gather.4
  179.3 63.3 all-gather.8
  244.2 61.9 all-gather.10
